TPU v7x, 512 devices: a whole 4x4x16 slice. The times are simulated.
512 devices in a mesh: fs: 64 (over z, y), tp: 8 (over x, core).
Axes of the slice: x: 4, y: 4, z: 16, core: 2. Of those that a mesh axis runs over, the one named last changes fastest.
Arguments:
- tokens: bfloat16 [49152, 2048], P('fs'), may hold values from -6 to 6
- norm_gain: float32 [2048], replicated, may hold values from 0.1 to 1.9
- up_weight: float32 [2048, 8192], P('fs', 'tp'), may hold values from -0.125 to 0.125
- up_scale: float32 [8192], P('tp'), may hold values from 0.5 to 2
- down_weight: float32 [8192, 2048], P('tp', 'fs'), may hold values from -0.0625 to 0.0625
- down_scale: float32 [2048], P('fs'), may hold values from 0.5 to 2
Outputs:
- output: bfloat16 [49152, 2048], P('fs', 'tp')
All inputs are finite; a program needn't handle non-finite values.
Results may differ from a plain program's by a relative error of at most 0.015.
Values may be sent and summed in bfloat16 or wider, within the bound.
No kernel may reach another device: no remote copies, remote signals or barrier semaphores. Data moves between devices by JAX's collectives and lax.ppermute only.
A program may use at most 64 MiB of HBM per device.

v0:
```python
import jax
import jax.numpy as jnp
from jax import lax
from jax.sharding import Mesh
from jax.sharding import PartitionSpec as P

FS = ("fs_0", "fs_1")
epsilon = 1e-06


def cut_along(array, dim, count):
    before, after = (array.shape[:dim], array.shape[dim + 1 :])
    return jnp.moveaxis(array.reshape(*before, count, -1, *after), dim, 0)


def summed_on_arrival(array, axis, dim):
    count = lax.axis_size(axis)
    tiles = lax.all_to_all(cut_along(array, dim, count), axis, 0, 0, tiled=True)
    return jnp.sum(tiles.astype(jnp.float32), axis=0)


def local(tokens, norm_gain, up_weight, up_scale, down_weight, down_scale):
    up_half = up_weight.astype(jnp.bfloat16)
    down_rows = (down_weight.T * down_scale[:, None]).astype(jnp.bfloat16)
    up_whole = lax.all_gather(up_half, FS, axis=0, tiled=True)
    down_whole = lax.all_gather(down_rows, FS, axis=0, tiled=True)
    floats = tokens.astype(jnp.float32)
    inverse = lax.rsqrt(jnp.mean(floats * floats, axis=-1, keepdims=True) + epsilon)
    normed = (floats * inverse * norm_gain).astype(jnp.bfloat16)
    up_pre = jnp.dot(normed, up_whole, preferred_element_type=jnp.float32)
    hidden = jnp.square(jax.nn.relu(up_pre * up_scale)).astype(jnp.bfloat16)
    hidden = lax.optimization_barrier(hidden)
    partial_value = lax.dot_general(
        hidden, down_whole, (((1,), (1,)), ((), ())), preferred_element_type=jnp.float32
    ).astype(jnp.bfloat16)
    return summed_on_arrival(partial_value, "tp", 1).astype(jnp.bfloat16)


def solution(mesh):
    split = Mesh(mesh.devices.reshape(16, 4, mesh.shape["tp"]), ("fs_0", "fs_1", "tp"))
    return jax.shard_map(
        local,
        mesh=split,
        in_specs=(P(FS, None), P(), P(FS, "tp"), P("tp"), P("tp", FS), P(FS)),
        out_specs=P(FS, "tp"),
        check_vma=False,
    )
```

profile of v0, /device:TPU:1, one launch (start us, length us, event | category | flops | bytes accessed | tf_op | source)
XLA Modules:
  0.0 362.0 jit_solution(8417288208690118681)
XLA Ops:
  6.5 0.0 copy-start
  6.5 0.0 copy-start.2
  6.5 0.0 copy-start.1
  6.5 0.0 all-gather.3.cloned.1.call-start
  6.5 1.7 convert_element_type.25
  8.2 0.0 all-gather.3.cloned.1.call-update
  8.3 0.0 all-gather.5.cloned.1.call-start
  8.3 1.6 fusion.9
  9.9 0.0 all-gather.5.cloned.1.call-update
  9.9 2.6 fusion
  12.5 140.0 %all-gather.3.cloned.1.call-done = bf16[2048,1024]{1,0:T(8,128)(2,1)} async-done(((bf16[32,1024]{1,0:T(8,128)(2,1)}), bf16[2048,1024]{1,0:T(8,128)(2,1)}) %all-gather.3.cloned.1.call-update) | async-done | bytes 4194320 | tf_op jit(solution)/shard_map/all_gather | solution.py:25
  152.5 0.0 copy-done
  152.5 0.0 copy-done.2
  152.5 0.0 copy-done.1
  152.6 6.9 %multiply_convert_fusion = bf16[768,1024]{1,0:T(8,128)(2,1)} fusion(bf16[2048,1024]{1,0:T(8,128)(2,1)} %all-gather.3.cloned.1.call-done, bf16[768,2048]{1,0:T(8,128)(2,1)S(1)} %copy-done, f32[2048]{0:T(1024)S(1)} %copy-done.1, f32[768]{0:T(1024)S(1)} %add_rsqrt_fusion, f32[1024]{0:T(1024)S(1)} %copy-done.2), kind=kOutput, calls=%fused_computation.8 | convolution fusion | flops 3230662656 | bytes 8928256 | tf_op jit(solution)/shard_map/dot_general | solution.py:30
  159.4 137.0 %all-gather.5.cloned.1.call-done = bf16[2048,1024]{1,0:T(8,128)(2,1)} async-done(((bf16[32,1024]{1,0:T(8,128)(2,1)}), bf16[2048,1024]{1,0:T(8,128)(2,1)}) %all-gather.5.cloned.1.call-update) | async-done | bytes 4194320 | tf_op jit(solution)/shard_map/all_gather | solution.py:26
  296.4 6.1 %convolution_convert_fusion = bf16[768,2048]{1,0:T(8,128)(2,1)S(1)} fusion(bf16[768,1024]{1,0:T(8,128)(2,1)} %multiply_convert_fusion, bf16[2048,1024]{1,0:T(8,128)(2,1)} %all-gather.5.cloned.1.call-done), kind=kOutput, calls=%fused_computation.5 | convolution fusion | flops 3222798336 | bytes 8912896 | tf_op jit(solution)/shard_map/dot_general | solution.py:33
  302.5 0.2 copy.10
  302.8 51.1 %all_to_all.5 = bf16[8,768,256]{2,1,0:T(8,128)(2,1)S(1)} all-to-all(bf16[8,768,256]{2,1,0:T(8,128)(2,1)S(1)} %bitcast.12), channel_id=1, replica_groups=mesh['fs_0'=16,'fs_1'=4,'tp'=8] {'tp'}, dimensions={0} | all-to-all | bytes 6291456 | tf_op jit(solution)/shard_map/all_to_all | solution.py:18
  353.9 1.3 reduce_sum.22
  (1 shorter events, 0.0 us)
Async XLA Ops:
  6.5 146.0 %copy-start = (bf16[768,2048]{1,0:T(8,128)(2,1)S(1)}, bf16[768,2048]{1,0:T(8,128)(2,1)}, u32[]{:S(2)}) copy-start(bf16[768,2048]{1,0:T(8,128)(2,1)} %param.6) | copy-start | bytes 9437188
  6.5 146.0 %copy-start.2 = (f32[1024]{0:T(1024)S(1)}, f32[1024]{0:T(1024)}, u32[]{:S(2)}) copy-start(f32[1024]{0:T(1024)} %param.9) | copy-start | bytes 12292
  6.5 146.0 %copy-start.1 = (f32[2048]{0:T(1024)S(1)}, f32[2048]{0:T(1024)}, u32[]{:S(2)}) copy-start(f32[2048]{0:T(1024)} %param.7) | copy-start | bytes 24580
  6.5 146.0 %all-gather.3.cloned.1.call-start = ((), (), s32[]{:S(2)}) async-start(), calls=%async_computation.1 | async-start | bytes 4259840 | tf_op jit(solution)/shard_map/all_gather | solution.py:25
  8.3 288.2 %all-gather.5.cloned.1.call-start = ((), (), s32[]{:S(2)}) async-start(), calls=%async_computation.2 | async-start | bytes 4259840 | tf_op jit(solution)/shard_map/all_gather | solution.py:26
Sparse Core Ops, SparseCore 0:
  10.3 142.2 all-gather.2
  155.5 140.8 all-gather.4
where the time goes:
time: 362 us
  waiting for transfers between devices  277 us (77%)
  blocking collectives  51.1 us (14%)
  between operations  13.4 us (4%)
  matrix products  13 us (4%)
  other arithmetic  7.15 us (2%)
    all_gather x1, waiting for transfers between devices, local(): up_whole = lax.all_gather(up_half, FS, axis=0, tiled=True)  140 us
    all_gather x1, waiting for transfers between devices, local(): down_whole = lax.all_gather(down_rows, FS, axis=0, tiled=True)  137 us
    all_to_all x1, blocking collectives, summed_on_arrival(): tiles = lax.all_to_all(cut_along(array, dim, count), axis, 0, 0, tiled=True)  51.1 us
  transfers between devices with their start and end apart: 2, of which 2 were waited for; matrix products, arithmetic and copies ran while one was open for 3% of the time, Pallas kernels for 0%

commit v1 on v0

--- a/solution.py
+++ b/solution.py
@@ -3,6 +3,7 @@
 from jax import lax
 from jax.sharding import Mesh
 from jax.sharding import PartitionSpec as P
+from jax.lax import all_gather
 
 FS = ("fs_0", "fs_1")
 epsilon = 1e-06
@@ -22,8 +23,11 @@
 def local(tokens, norm_gain, up_weight, up_scale, down_weight, down_scale):
     up_half = up_weight.astype(jnp.bfloat16)
     down_rows = (down_weight.T * down_scale[:, None]).astype(jnp.bfloat16)
-    up_whole = lax.all_gather(up_half, FS, axis=0, tiled=True)
-    down_whole = lax.all_gather(down_rows, FS, axis=0, tiled=True)
+    up_whole, down_whole = jnp.split(
+        all_gather(jnp.concatenate([up_half, down_rows], 1), FS, axis=0, tiled=True),
+        [up_half.shape[1]],
+        1,
+    )
     floats = tokens.astype(jnp.float32)
     inverse = lax.rsqrt(jnp.mean(floats * floats, axis=-1, keepdims=True) + epsilon)
     normed = (floats * inverse * norm_gain).astype(jnp.bfloat16)

time: 362 us -> 232 us (0.64)
  waiting for transfers between devices: 277 us -> 152 us
    all_gather x2 -> x1, waiting for transfers between devices: 277 us -> 152 us  [local(): all_gather(jnp.concatenate([up_half, down_rows], 1), FS, axis=0, tiled=True)]
  transfers between devices with their start and end apart: 2 -> 1, of which waited for: 2 -> 1; matrix products, arithmetic and copies ran while one was open for 3% -> 1% of each run, Pallas kernels for 0% -> 0%
where the time goes in v1:
time: 232 us
  waiting for transfers between devices  152 us (66%)
  blocking collectives  49.9 us (22%)
  between operations  13.4 us (6%)
  matrix products  9.51 us (4%)
  other arithmetic  6.57 us (3%)
    all_gather x1, waiting for transfers between devices, local(): all_gather(jnp.concatenate([up_half, down_rows], 1), FS, axis=0, tiled=True)  152 us
    all_to_all x1, blocking collectives, summed_on_arrival(): tiles = lax.all_to_all(cut_along(array, dim, count), axis, 0, 0, tiled=True)  49.9 us
    dot_general x1, matrix products, local(): up_pre = jnp.dot(normed, up_whole, preferred_element_type=jnp.float32)  5.8 us
  transfers between devices with their start and end apart: 1, of which 1 were waited for; matrix products, arithmetic and copies ran while one was open for 1% of the time, Pallas kernels for 0%

profile of v1, /device:TPU:1, one launch (start us, length us, event | category | flops | bytes accessed | tf_op | source)
XLA Modules:
  0.0 231.7 jit_solution(5611939754312704504)
XLA Ops:
  6.5 0.0 copy-start
  6.5 0.0 copy-start.3
  6.5 0.0 copy-start.2
  6.5 0.0 all-gather.2.cloned.1.call-start
  6.5 1.1 convert_element_type.25
  7.6 1.0 fusion.17
  8.6 0.7 pad_maximum_fusion
  9.3 0.0 all-gather.2.cloned.1.call-update
  9.3 2.6 %fusion = f32[768]{0:T(1024)S(1)} fusion(bf16[768,2048]{1,0:T(8,128)(2,1)} %param.6), kind=kLoop, calls=%fused_computation.2 | loop fusion | flops 4717824 | bytes 3148800 | tf_op jit(solution)/shard_map/reduce_sum | solution.py:32
  11.9 152.1 %all-gather.2.cloned.1.call-done = bf16[2048,2048]{1,0:T(8,128)(2,1)} async-done(((bf16[32,2048]{1,0:T(8,128)(2,1)}), bf16[2048,2048]{1,0:T(8,128)(2,1)}) %all-gather.2.cloned.1.call-update) | async-done | bytes 8388624 | tf_op jit(solution)/shard_map/all_gather | solution.py:27
  164.0 0.0 copy-done
  164.0 0.0 copy-done.3
  164.0 0.0 copy-done.2
  164.0 0.0 copy-start.1
  164.0 5.8 %multiply_convert_fusion = bf16[768,1024]{1,0:T(8,128)(2,1)S(1)} fusion(bf16[2048,2048]{1,0:T(8,128)(2,1)} %all-gather.2.cloned.1.call-done, bf16[768,2048]{1,0:T(8,128)(2,1)S(1)} %copy-done, f32[2048]{0:T(1024)S(1)} %copy-done.2, f32[768]{0:T(1024)S(1)} %add_rsqrt_fusion, f32[1024]{0:T(1024)S(1)} %copy-done.3), kind=kOutput, calls=%fused_computation.11 | convolution fusion | flops 3230662656 | bytes 8928256 | tf_op jit(solution)/shard_map/dot_general | solution.py:34
  169.8 0.0 copy-done.1
  169.8 3.7 %fusion.7 = bf16[768,2048]{1,0:T(8,128)(2,1)S(1)} fusion(bf16[768,1024]{1,0:T(8,128)(2,1)S(1)} %multiply_convert_fusion, bf16[2048,2048]{1,0:T(8,128)(2,1)S(1)} %copy-done.1), kind=kOutput, calls=%fused_computation.9 | convolution fusion | flops 3222798336 | bytes 8912896 | tf_op jit(solution)/shard_map/dot_general | solution.py:37
  173.5 0.2 copy.10
  173.7 49.9 %all_to_all.5 = bf16[8,768,256]{2,1,0:T(8,128)(2,1)S(1)} all-to-all(bf16[8,768,256]{2,1,0:T(8,128)(2,1)S(1)} %bitcast.10), channel_id=1, replica_groups=mesh['fs_0'=16,'fs_1'=4,'tp'=8] {'tp'}, dimensions={0} | all-to-all | bytes 6291456 | tf_op jit(solution)/shard_map/all_to_all | solution.py:19
  223.6 1.3 reduce_sum.22
  (1 shorter events, 0.0 us)
Async XLA Ops:
  6.5 157.4 %copy-start = (bf16[768,2048]{1,0:T(8,128)(2,1)S(1)}, bf16[768,2048]{1,0:T(8,128)(2,1)}, u32[]{:S(2)}) copy-start(bf16[768,2048]{1,0:T(8,128)(2,1)} %param.6) | copy-start | bytes 9437188
  6.5 157.4 %copy-start.3 = (f32[1024]{0:T(1024)S(1)}, f32[1024]{0:T(1024)}, u32[]{:S(2)}) copy-start(f32[1024]{0:T(1024)} %param.9) | copy-start | bytes 12292
  6.5 157.4 %copy-start.2 = (f32[2048]{0:T(1024)S(1)}, f32[2048]{0:T(1024)}, u32[]{:S(2)}) copy-start(f32[2048]{0:T(1024)} %param.7) | copy-start | bytes 24580
  6.5 157.4 %all-gather.2.cloned.1.call-start = ((), (), s32[]{:S(2)}) async-start(), calls=%async_computation.1 | async-start | bytes 8519680 | tf_op jit(solution)/shard_map/all_gather | solution.py:27
  164.0 5.8 %copy-start.1 = (bf16[2048,2048]{1,0:T(8,128)(2,1)S(1)}, bf16[2048,2048]{1,0:T(8,128)(2,1)}, u32[]{:S(2)}) copy-start(bf16[2048,2048]{1,0:T(8,128)(2,1)} %all-gather.2.cloned.1.call-done) | copy-start | bytes 25165828
Sparse Core Ops, SparseCore 0:
  10.3 153.6 all-gather.1

commit v2 on v0

--- a/solution.py
+++ b/solution.py
@@ -1,11 +1,21 @@
+import functools
 import jax
 import jax.numpy as jnp
 from jax import lax
 from jax.sharding import Mesh
 from jax.sharding import PartitionSpec as P
+from jax.lax import all_to_all, axis_size
 
 FS = ("fs_0", "fs_1")
 epsilon = 1e-06
+
+
+def name_tiles_all(point, across):
+    o_now = jnp.concatenate(all_to_all(jnp.stack(axis_size(across) * [point]), across, 0, 0), 0)
+    return o_now
+
+
+choose_the_pipes = functools.partial(name_tiles_all, across=FS)
 
 
 def cut_along(array, dim, count):
@@ -22,7 +32,7 @@
 def local(tokens, norm_gain, up_weight, up_scale, down_weight, down_scale):
     up_half = up_weight.astype(jnp.bfloat16)
     down_rows = (down_weight.T * down_scale[:, None]).astype(jnp.bfloat16)
-    up_whole = lax.all_gather(up_half, FS, axis=0, tiled=True)
+    up_whole = choose_the_pipes(up_half)
     down_whole = lax.all_gather(down_rows, FS, axis=0, tiled=True)
     floats = tokens.astype(jnp.float32)
     inverse = lax.rsqrt(jnp.mean(floats * floats, axis=-1, keepdims=True) + epsilon)

time: 362 us -> 307 us (0.85)
  waiting for transfers between devices: 277 us -> 205 us
  starting transfers between devices: 0.04 us -> 19.8 us
    all_to_all x0 -> x1, waiting for transfers between devices: none -> 205 us  [name_tiles_all(): all_to_all(jnp.stack(axis_size(across) * [point]), across, 0, 0)]
    all_gather x1 -> x0, waiting for transfers between devices: 140 us -> none  [local(): up_whole = lax.all_gather(up_half, FS, axis=0, tiled=True)]
    all_gather x1, waiting for transfers between devices: 137 us -> 0.01 us  [local(): down_whole = lax.all_gather(down_rows, FS, axis=0, tiled=True)]
    all_to_all x0 -> x1, starting transfers between devices: none -> 19.8 us  [name_tiles_all(): all_to_all(jnp.stack(axis_size(across) * [point]), across, 0, 0)]
  transfers between devices with their start and end apart: 2 -> 2, of which waited for: 2 -> 1; matrix products, arithmetic and copies ran while one was open for 3% -> 3% of each run, Pallas kernels for 0% -> 0%
where the time goes in v2:
time: 307 us
  waiting for transfers between devices  205 us (67%)
  blocking collectives  49.3 us (16%)
  starting transfers between devices  19.8 us (6%)
  between operations  13.5 us (4%)
  matrix products  13 us (4%)
  other arithmetic  3.59 us (1%)
    all_to_all x1, waiting for transfers between devices, name_tiles_all(): all_to_all(jnp.stack(axis_size(across) * [point]), across, 0, 0)  205 us
    all_to_all x1, blocking collectives, summed_on_arrival(): tiles = lax.all_to_all(cut_along(array, dim, count), axis, 0, 0, tiled=True)  49.3 us
    all_to_all x1, starting transfers between devices, name_tiles_all(): all_to_all(jnp.stack(axis_size(across) * [point]), across, 0, 0)  19.8 us
    dot_general x1, matrix products, local(): up_pre = jnp.dot(normed, up_whole, preferred_element_type=jnp.float32)  6.88 us
  transfers between devices with their start and end apart: 2, of which 1 were waited for; matrix products, arithmetic and copies ran while one was open for 3% of the time, Pallas kernels for 0%

profile of v2, /device:TPU:1, one launch (start us, length us, event | category | flops | bytes accessed | tf_op | source)
XLA Modules:
  0.0 306.6 jit_solution(12106306585804745655)
XLA Ops:
  6.5 0.9 convert_element_type.25
  7.4 2.5 stack.2
  9.9 0.0 copy-start.1
  9.9 0.0 copy-start.2
  9.9 0.0 copy-start
  9.9 19.8 %all-to-all-start = ((bf16[64,32,1024]{2,1,0:T(8,128)(2,1)}), bf16[64,32,1024]{2,1,0:T(8,128)(2,1)}, u32[]{:S(2)}, u32[]{:S(2)}) async-start(bf16[64,32,1024]{2,1,0:T(8,128)(2,1)} %stack.2), calls=%async_computation | async-start | bytes 8388608 | tf_op jit(solution)/shard_map/all_to_all | solution.py:14
  29.7 0.0 copy-start.3
  29.7 0.0 copy-start.4
  29.8 0.0 all-gather.2.cloned.1.call-start
  29.8 0.0 copy-done.1
  29.8 0.0 copy-done.2
  29.8 0.7 fusion.9
  30.5 0.0 all-gather.2.cloned.1.call-update
  30.6 0.0 copy-done
  30.6 0.7 fusion
  31.3 204.7 %all-to-all-done = bf16[64,32,1024]{2,1,0:T(8,128)(2,1)} async-done(((bf16[64,32,1024]{2,1,0:T(8,128)(2,1)}), bf16[64,32,1024]{2,1,0:T(8,128)(2,1)}, u32[]{:S(2)}, u32[]{:S(2)}) %all-to-all-start) | async-done | bytes 4194336 | tf_op jit(solution)/shard_map/all_to_all | solution.py:14
  236.0 0.0 copy-done.3
  236.0 0.0 copy-done.4
  236.0 6.9 %multiply_convert_fusion = bf16[768,1024]{1,0:T(8,128)(2,1)} fusion(bf16[2048,1024]{1,0:T(8,128)(2,1)} %bitcast, bf16[768,2048]{1,0:T(8,128)(2,1)S(1)} %copy-done, f32[2048]{0:T(1024)S(1)} %copy-done.3, f32[768]{0:T(1024)S(1)} %add_rsqrt_fusion, f32[1024]{0:T(1024)S(1)} %copy-done.4), kind=kOutput, calls=%fused_computation.8 | convolution fusion | flops 3230662656 | bytes 8928256 | tf_op jit(solution)/shard_map/dot_general | solution.py:40
  242.9 0.0 all-gather.2.cloned.1.call-done
  242.9 6.1 %convolution_convert_fusion = bf16[768,2048]{1,0:T(8,128)(2,1)S(1)} fusion(bf16[768,1024]{1,0:T(8,128)(2,1)} %multiply_convert_fusion, bf16[2048,1024]{1,0:T(8,128)(2,1)} %all-gather.2.cloned.1.call-done), kind=kOutput, calls=%fused_computation.5 | convolution fusion | flops 3222798336 | bytes 8912896 | tf_op jit(solution)/shard_map/dot_general | solution.py:43
  249.0 0.2 copy.10
  249.2 49.3 %all_to_all.10 = bf16[8,768,256]{2,1,0:T(8,128)(2,1)S(1)} all-to-all(bf16[8,768,256]{2,1,0:T(8,128)(2,1)S(1)} %bitcast.13), channel_id=1, replica_groups=mesh['fs_0'=16,'fs_1'=4,'tp'=8] {'tp'}, dimensions={0} | all-to-all | bytes 6291456 | tf_op jit(solution)/shard_map/all_to_all | solution.py:28
  298.5 1.3 reduce_sum.22
  (1 shorter events, 0.0 us)
Async XLA Ops:
  9.9 19.9 %copy-start.1 = (f32[1024,32]{0,1:T(8,128)S(1)}, f32[1024,32]{0,1:T(8,128)}, u32[]{:S(2)}) copy-start(f32[1024,32]{0,1:T(8,128)} %param.10) | copy-start | bytes 393220
  9.9 19.9 %copy-start.2 = (f32[32]{0:T(128)S(1)}, f32[32]{0:T(128)}, u32[]{:S(2)}) copy-start(f32[32]{0:T(128)} %param.11) | copy-start | bytes 388
  9.9 20.6 %copy-start = (bf16[768,2048]{1,0:T(8,128)(2,1)S(1)}, bf16[768,2048]{1,0:T(8,128)(2,1)}, u32[]{:S(2)}) copy-start(bf16[768,2048]{1,0:T(8,128)(2,1)} %param.6) | copy-start | bytes 9437188
  9.9 226.0 %all-to-all-start = ((bf16[64,32,1024]{2,1,0:T(8,128)(2,1)}), bf16[64,32,1024]{2,1,0:T(8,128)(2,1)}, u32[]{:S(2)}, u32[]{:S(2)}) async-start(bf16[64,32,1024]{2,1,0:T(8,128)(2,1)} %stack.2), calls=%async_computation | async-start | bytes 8388608 | tf_op jit(solution)/shard_map/all_to_all | solution.py:14
  29.7 206.2 %copy-start.3 = (f32[2048]{0:T(1024)S(1)}, f32[2048]{0:T(1024)}, u32[]{:S(2)}) copy-start(f32[2048]{0:T(1024)} %param.7) | copy-start | bytes 24580
  29.7 206.2 %copy-start.4 = (f32[1024]{0:T(1024)S(1)}, f32[1024]{0:T(1024)}, u32[]{:S(2)}) copy-start(f32[1024]{0:T(1024)} %param.9) | copy-start | bytes 12292
  29.8 213.1 %all-gather.2.cloned.1.call-start = ((), (), s32[]{:S(2)}) async-start(), calls=%async_computation.2 | async-start | bytes 4259840 | tf_op jit(solution)/shard_map/all_gather | solution.py:36
Sparse Core Ops, SparseCore 0:
  33.5 208.8 all-gather.1
